TPU v7x, 32 devices: a whole 2x2x4 slice. The times are simulated.
32 devices in a mesh: dp: 4 (over y, x), kv: 4 (over z), tp: 2 (over core).
Axes of the slice: x: 2, y: 2, z: 4, core: 2. Of those that a mesh axis runs over, the one named last changes fastest.
Arguments:
- tokens: bfloat16 [16, 4096], P('dp', ('kv', 'tp')), may hold values from -24 to 24
- rec_state: float32 [16, 16, 128, 128], P(('dp', 'kv'), 'tp'), may hold values from -2 to 2
- norm_gain: float32 [4096], replicated, may hold values from 0.1 to 1.9
- w_query: bfloat16 [4096, 2048], P('kv', 'tp'), may hold values from -0.09375 to 0.09375
- w_forget: bfloat16 [4096, 2048], P('kv', 'tp'), may hold values from -0.09375 to 0.09375
- w_input: bfloat16 [4096, 2048], P('kv', 'tp'), may hold values from -0.09375 to 0.09375
- w_outgate: bfloat16 [4096, 2048], P('kv', 'tp'), may hold values from -0.09375 to 0.09375
- lower_bound: float32 [2048], P('tp'), may hold values from 0 to 0.9
- head_gain: float32 [2048], P('tp'), may hold values from 0.1 to 1.9
- w_heads_out: bfloat16 [2048, 4096], P(None, ('kv', 'tp')), may hold values from -0.125 to 0.125
- mixer_gain: float32 [4096], replicated, may hold values from 0.1 to 1.9
- w_gate: bfloat16 [4096, 11264], P(None, ('kv', 'tp')), may hold values from -0.09375 to 0.09375
- w_up: bfloat16 [4096, 11264], P(None, ('kv', 'tp')), may hold values from -0.09375 to 0.09375
- w_down: bfloat16 [11264, 4096], P(('kv', 'tp')), may hold values from -0.078125 to 0.078125
Outputs:
- result: bfloat16 [16, 4096], P('dp', ('kv', 'tp'))
- new_state: float32 [16, 16, 128, 128], P(('dp', 'kv'), 'tp')
All inputs are finite; a program needn't handle non-finite values.
Results may differ from a plain program's by a relative error of at most 0.012.
Values may be sent and summed in bfloat16 or wider, within the bound.
A program may use at most 128 MiB of HBM per device.

v0:
```python
import jax
import jax.numpy as jnp
from jax import lax
from jax.sharding import PartitionSpec as P

HEAD_DIM = 128
epsilon = 1e-06


def channel_mixer(whole_rows, mixer_gain, w_gate, w_up, w_down):
    rows_float = whole_rows.astype(jnp.float32)
    mixer_scale = lax.rsqrt(jnp.mean(rows_float * rows_float, axis=1, keepdims=True) + epsilon)
    normed = (rows_float * mixer_scale * mixer_gain).astype(jnp.bfloat16)
    gate_val = jnp.dot(normed, w_gate, preferred_element_type=jnp.float32)
    up_val = jnp.dot(normed, w_up, preferred_element_type=jnp.float32)
    hidden = (jax.nn.silu(gate_val) * up_val).astype(jnp.bfloat16)
    return jnp.dot(hidden, w_down, preferred_element_type=jnp.float32)


def local(
    tokens,
    rec_state,
    norm_gain,
    w_query,
    w_forget,
    w_input,
    w_outgate,
    lower_bound,
    head_gain,
    w_heads_out,
    mixer_gain,
    w_gate,
    w_up,
    w_down,
):
    kv_count = lax.axis_size("kv")
    tp_count = lax.axis_size("tp")
    kv_index = lax.axis_index("kv")
    row_count = tokens.shape[0]
    seq_count = rec_state.shape[0]
    model_width = norm_gain.shape[0]
    col_block = model_width // kv_count
    tok_float = tokens.astype(jnp.float32)
    whole_rows = lax.all_gather(tokens, ("kv", "tp"), axis=1, tiled=True).astype(jnp.float32)
    squares = jnp.sum(whole_rows * whole_rows, axis=1)
    own_cols = lax.dynamic_slice_in_dim(whole_rows, kv_index * col_block, col_block, 1)
    gain_block = lax.dynamic_slice_in_dim(norm_gain, kv_index * col_block, col_block, 0)
    scaled = (own_cols * gain_block).astype(jnp.bfloat16)
    projected = lax.psum_scatter(
        jnp.stack(
            [
                jnp.dot(scaled, weight, preferred_element_type=jnp.float32)
                for weight in (w_query, w_forget, w_input, w_outgate)
            ],
            axis=1,
        ),
        "kv",
        scatter_dimension=0,
        tiled=True,
    )
    my_squares = lax.dynamic_slice_in_dim(squares, kv_index * seq_count, seq_count, 0)
    row_scale = lax.rsqrt(my_squares / model_width + epsilon)[:, None]
    query_pre = row_scale * projected[:, 0]
    forget_pre = row_scale * projected[:, 1]
    value_in = row_scale * projected[:, 2]
    gate_pre = row_scale * projected[:, 3]
    forget = lower_bound + (1.0 - lower_bound) * jax.nn.sigmoid(forget_pre)
    key_in = 1.0 - forget
    query_act = jax.nn.silu(query_pre)
    head_count = rec_state.shape[1]
    shaped = (seq_count, head_count, HEAD_DIM)
    forget = forget.reshape(shaped)
    key_in = key_in.reshape(shaped)
    value_in = value_in.reshape(shaped)
    query_act = query_act.reshape(shaped)
    new_state = forget[:, :, :, None] * rec_state + key_in[:, :, :, None] * value_in[:, :, None, :]
    head_out = jnp.sum(query_act[:, :, :, None] * new_state, axis=2)
    head_out = head_out * lax.rsqrt(jnp.mean(head_out * head_out, axis=2, keepdims=True) + epsilon)
    head_out = head_out * head_gain.reshape(head_count, HEAD_DIM)
    local_width = head_count * HEAD_DIM
    gated = (head_out.reshape(seq_count, local_width) * jax.nn.silu(gate_pre)).astype(jnp.bfloat16)
    every_head = lax.all_gather(gated[None], ("kv", "tp"), axis=0, tiled=True)
    every_head = every_head.reshape(kv_count, tp_count, seq_count, local_width)
    every_head = every_head.transpose(0, 2, 1, 3).reshape(
        kv_count * seq_count, tp_count * local_width
    )
    mixed_add = jnp.dot(every_head, w_heads_out, preferred_element_type=jnp.float32)
    mixed = (tok_float + mixed_add).astype(jnp.bfloat16)
    gathered = lax.all_gather(mixed, ("kv", "tp"), axis=1, tiled=True)
    terms = channel_mixer(gathered, mixer_gain, w_gate, w_up, w_down)
    out_block = model_width // (kv_count * tp_count)
    blocked = terms.reshape(row_count, kv_count, tp_count, out_block)
    chip_sum = lax.psum_scatter(blocked.astype(jnp.bfloat16), "tp", scatter_dimension=2, tiled=True)
    down_sum = (
        lax.psum_scatter(chip_sum, "kv", scatter_dimension=1, tiled=True)
        .astype(jnp.float32)
        .reshape(row_count, out_block)
    )
    result = (mixed.astype(jnp.float32) + down_sum).astype(jnp.bfloat16)
    return (result, new_state)


def solution(mesh):
    placed = (
        P("dp", ("kv", "tp")),
        P(("dp", "kv"), "tp", None, None),
        P(),
        P("kv", "tp"),
        P("kv", "tp"),
        P("kv", "tp"),
        P("kv", "tp"),
        P("tp"),
        P("tp"),
        P(None, ("kv", "tp")),
        P(),
        P(None, ("kv", "tp")),
        P(None, ("kv", "tp")),
        P(("kv", "tp"), None),
    )
    return jax.shard_map(
        local,
        mesh=mesh,
        in_specs=placed,
        out_specs=(P("dp", ("kv", "tp")), P(("dp", "kv"), "tp", None, None)),
        check_vma=False,
    )
```

profile of v0, /device:TPU:0, one launch (start us, length us, event | category | flops | bytes accessed | tf_op | source)
XLA Modules:
  0.0 140.6 jit_solution(1454577620565583170)
XLA Ops:
  7.2 16.1 %all_gather.9 = bf16[4,4096]{1,0:T(4,128)(2,1)S(1)} all-gather(bf16[4,512]{1,0:T(4,128)(2,1)} %param.14), channel_id=1, replica_groups=mesh['dp'=4,'kv'=4,'tp'=2] {'kv','tp'}, dimensions={1}, use_global_device_ids=true | all-gather | bytes 36864 | tf_op jit(solution)/shard_map/all_gather | solution.py:44
  23.3 0.8 dynamic_slice.11
  24.2 0.4 convolution_bitcast_fusion
  24.6 0.3 copy-done.1
  24.9 0.4 convolution_bitcast_fusion.1
  25.3 0.6 copy-done.2
  25.9 0.4 convolution_bitcast_fusion.2
  26.7 0.4 convolution_bitcast_fusion.3
  27.1 0.7 copy.18
  27.8 0.6 dynamic-slice.2
  28.4 0.6 dynamic-slice
  29.1 0.6 dynamic_slice.9
  30.4 32.8 %all-reduce.5.cloned.1.call-done = f32[4,4,1024]{2,1,0:T(4,128)} async-done(((f32[4,4,1024]{2,1,0:T(4,128)}), f32[4,4,1024]{2,1,0:T(4,128)}) %all-reduce.5.cloned.1.call-update) | async-done | bytes 65552
  63.2 1.5 %dynamic-slice_multiply_fusion = (f32[1,1,1024]{2,1,0:T(1,128)S(1)}, f32[1,1,1024]{2,1,0:T(1,128)S(1)}, f32[1,1,1024]{2,1,0:T(1,128)S(1)}, f32[1,1,1024]{2,1,0:T(1,128)S(1)}) fusion(f32[4,4,1024]{2,1,0:T(4,128)} %all-reduce.5.cloned.1.call-done, u32[]{:T(128)} %bitcast.19, u32[]{:T(128)S(6)} %convert.4, f32[]{:T(128)} %bitcast, u32[]{:T(128)S(6)} %convert.3, ...), kind=kLoop, calls=%fused_computation.26 | loop fusion | flops 7168 | bytes 32788 | tf_op jit(solution)/shard_map/mul | solution.py:66
  64.8 1.3 multiply_reduce_fusion
  66.2 12.8 %all-gather = bf16[8192]{0:T(1024)(128)(2,1)S(1)} all-gather(bf16[1024]{0:T(1024)(128)(2,1)S(1)} %fusion.13), channel_id=2, replica_groups=mesh['dp'=4,'kv'=4,'tp'=2] {'kv','tp'}, dimensions={0}, use_global_device_ids=true | all-gather | bytes 18432 | tf_op jit(solution)/shard_map/all_gather | solution.py:82
  79.0 2.0 %fusion.1 = bf16[4,512]{1,0:T(4,128)(2,1)S(1)} fusion(bf16[4,2048]{1,0:T(4,128)(2,1)S(1)} %reshape_transpose_reshape.3, bf16[2048,512]{1,0:T(8,128)(2,1)} %param.23, bf16[4,512]{1,0:T(4,128)(2,1)S(1)} %copy-done.6), kind=kOutput, calls=%fused_computation.8 | convolution fusion | flops 8394752 | bytes 2121728 | tf_op jit(solution)/shard_map/dot_general | solution.py:87
  81.0 14.1 %all_gather.11 = bf16[4,4096]{1,0:T(4,128)(2,1)S(1)} all-gather(bf16[4,512]{1,0:T(4,128)(2,1)S(1)} %fusion.1), channel_id=1, replica_groups=mesh['dp'=4,'kv'=4,'tp'=2] {'kv','tp'}, dimensions={1}, use_global_device_ids=true | all-gather | bytes 36864 | tf_op jit(solution)/shard_map/all_gather | solution.py:89
  95.2 5.9 %fusion.18 = f32[4,1408]{1,0:T(4,128)S(1)} fusion(bf16[4096,1408]{1,0:T(8,128)(2,1)} %param.25, bf16[4,4096]{1,0:T(4,128)(2,1)S(1)} %all_gather.11, f32[4096]{0:T(1024)S(1)} %copy-done.5, f32[4]{0:T(128)S(1)} %add_rsqrt_fusion), kind=kOutput, calls=%fused_computation.45 | convolution fusion | flops 46202880 | bytes 11606032 | tf_op jit(solution)/shard_map/dot_general | solution.py:14
  101.1 11.0 %convolution_convert_fusion = bf16[4,4096]{1,0:T(4,128)(2,1)S(1)} fusion(bf16[1408,4096]{1,0:T(8,128)(2,1)} %param.27, bf16[4096,1408]{1,0:T(8,128)(2,1)} %param.26, f32[4,1408]{1,0:T(4,128)S(1)} %fusion.18, bf16[4,4096]{1,0:T(4,128)(2,1)S(1)} %all_gather.11, f32[4096]{0:T(1024)S(1)} %copy-done.5, f32[4]{0:T(128)S(1)} %add_rsqrt_fusion), kind=kOutput, calls=%fused_computation | convolution fusion | flops 92390400 | bytes 23173136 | tf_op jit(solution)/shard_map/dot_general | solution.py:17
  112.1 3.6 %all-reduce.1 = bf16[4,4,2,512]{3,0,2,1:T(4,128)(2,1)S(1)} all-reduce(bf16[4,4,2,512]{3,0,2,1:T(4,128)(2,1)S(1)} %bitcast.49), channel_id=4, replica_groups=mesh['dp'=4,'kv'=4,'tp'=2] {'tp'}, use_global_device_ids=true, to_apply=%region_5.6.clone | all-reduce | flops 16384 | bytes 65536
  115.7 0.6 constant_dynamic-slice_fusion
  116.4 16.2 %all-reduce.2 = bf16[4,4,1,512]{3,0,2,1:T(4,128)(2,1)S(1)} all-reduce(bf16[4,4,1,512]{3,0,2,1:T(4,128)(2,1)S(1)} %constant_dynamic-slice_fusion), channel_id=5, replica_groups=mesh['dp'=4,'kv'=4,'tp'=2] {'kv'}, use_global_device_ids=true, to_apply=%region_6.7.clone | all-reduce | flops 8192 | bytes 32768
  132.6 1.2 fusion.9
  (35 shorter events, 1.0 us)
Async XLA Ops:
  7.2 17.0 %copy-start = (bf16[1024,1024]{1,0:T(8,128)(2,1)S(1)}, bf16[1024,1024]{1,0:T(8,128)(2,1)}, u32[]{:S(2)}) copy-start(bf16[1024,1024]{1,0:T(8,128)(2,1)} %param.20) | copy-start | bytes 6291460
  7.2 56.0 %all-reduce.5.cloned.1.call-start = ((), (), s32[]{:S(2)}) async-start(), calls=%async_computation | async-start | bytes 131072
  23.3 1.6 %copy-start.1 = (bf16[1024,1024]{1,0:T(8,128)(2,1)S(1)}, bf16[1024,1024]{1,0:T(8,128)(2,1)}, u32[]{:S(2)}) copy-start(bf16[1024,1024]{1,0:T(8,128)(2,1)} %param.19) | copy-start | bytes 6291460
  24.2 1.8 %copy-start.2 = (bf16[1024,1024]{1,0:T(8,128)(2,1)S(1)}, bf16[1024,1024]{1,0:T(8,128)(2,1)}, u32[]{:S(2)}) copy-start(bf16[1024,1024]{1,0:T(8,128)(2,1)} %param.18) | copy-start | bytes 6291460
  24.9 1.7 %copy-start.3 = (bf16[1024,1024]{1,0:T(8,128)(2,1)S(1)}, bf16[1024,1024]{1,0:T(8,128)(2,1)}, u32[]{:S(2)}) copy-start(bf16[1024,1024]{1,0:T(8,128)(2,1)} %param.17) | copy-start | bytes 6291460
  25.9 1.8 %copy-start.10 = (u32[32]{0:T(128)S(1)}, u32[32]{0:T(128)}, u32[]{:S(2)}) copy-start(u32[32]{0:T(128)} %constant.45) | copy-start | bytes 388
  25.9 2.4 %copy-start.9 = (u32[32]{0:T(128)S(1)}, u32[32]{0:T(128)}, u32[]{:S(2)}) copy-start(u32[32]{0:T(128)} %constant.41) | copy-start | bytes 388
  25.9 38.8 %copy-start.7 = (f32[1024]{0:T(1024)S(1)}, f32[1024]{0:T(1024)}, u32[]{:S(2)}) copy-start(f32[1024]{0:T(1024)} %param.21) | copy-start | bytes 12292
  25.9 38.8 %copy-start.4 = (f32[1,8,128,128]{3,2,1,0:T(8,128)S(1)}, f32[1,8,128,128]{3,2,1,0:T(8,128)}, u32[]{:S(2)}) copy-start(f32[1,8,128,128]{3,2,1,0:T(8,128)} %param.15) | copy-start | bytes 1572868
  26.6 39.6 %copy-start.8 = (f32[1024]{0:T(1024)S(1)}, f32[1024]{0:T(1024)}, u32[]{:S(2)}) copy-start(f32[1024]{0:T(1024)} %param.22) | copy-start | bytes 12292
  26.7 52.4 %copy-start.6 = (bf16[4,512]{1,0:T(4,128)(2,1)S(1)}, bf16[4,512]{1,0:T(4,128)(2,1)}, u32[]{:S(2)}) copy-start(bf16[4,512]{1,0:T(4,128)(2,1)} %param.14) | copy-start | bytes 12292
  27.0 68.2 %copy-start.5 = (f32[4096]{0:T(1024)S(1)}, f32[4096]{0:T(1024)}, u32[]{:S(2)}) copy-start(f32[4096]{0:T(1024)} %param.24) | copy-start | bytes 49156
Sparse Core Ops, SparseCore 0:
  27.9 35.2 all-reduce.4
where the time goes:
time: 141 us
  blocking collectives  62.7 us (44%)
  waiting for transfers between devices  32.8 us (23%)
  matrix products  20.4 us (14%)
  between operations  14.9 us (11%)
  local copies, waits for them, and re-layouts  5.37 us (4%)
  other arithmetic  4.46 us (3%)
    unnamed x2, waiting for transfers between devices  32.8 us
    unnamed x2, blocking collectives  19.8 us
    all_gather x1, blocking collectives, local(): lax.all_gather(tokens, ('kv', 'tp'), axis=1, tiled=True).astype(jnp.float32)  16.1 us
    all_gather x1, blocking collectives, local(): gathered = lax.all_gather(mixed, ('kv', 'tp'), axis=1, tiled=True)  14.1 us
    all_gather x1, blocking collectives, local(): every_head = lax.all_gather(gated[None], ('kv', 'tp'), axis=0, tiled=True)  12.8 us
    dot_general x1, matrix products, channel_mixer(): return jnp.dot(hidden, w_down, preferred_element_type=jnp.float32)  11 us
    dot_general x1, matrix products, channel_mixer(): gate_val = jnp.dot(normed, w_gate, preferred_element_type=jnp.float32)  5.9 us
    unnamed x25, local copies, waits for them, and re-layouts  3.18 us
  transfers between devices with their start and end apart: 1, of which 1 were waited for; matrix products, arithmetic and copies ran while one was open for 1% of the time, Pallas kernels for 0%

commit v1 on v0

--- a/solution.py
+++ b/solution.py
@@ -41,7 +41,10 @@
     model_width = norm_gain.shape[0]
     col_block = model_width // kv_count
     tok_float = tokens.astype(jnp.float32)
-    whole_rows = lax.all_gather(tokens, ("kv", "tp"), axis=1, tiled=True).astype(jnp.float32)
+    whole_rows = jnp.concatenate(
+        lax.all_to_all(jnp.stack([tokens] * lax.axis_size(("kv", "tp"))), ("kv", "tp"), 0, 0),
+        axis=1,
+    ).astype(jnp.float32)
     squares = jnp.sum(whole_rows * whole_rows, axis=1)
     own_cols = lax.dynamic_slice_in_dim(whole_rows, kv_index * col_block, col_block, 1)
     gain_block = lax.dynamic_slice_in_dim(norm_gain, kv_index * col_block, col_block, 0)

time: 141 us -> 136 us (0.965)
  blocking collectives: 62.7 us -> 46.6 us
  starting transfers between devices: 0.04 us -> 6.39 us
  local copies, waits for them, and re-layouts: 5.37 us -> 8.81 us
  waiting for transfers between devices: 32.8 us -> 34.5 us
    all_gather x1 -> x0, blocking collectives: 16.1 us -> none  [local(): lax.all_gather(tokens, ('kv', 'tp'), axis=1, tiled=True).astype(jnp.float32)]
    all_to_all x0 -> x1, starting transfers between devices: none -> 6.35 us  [local(): lax.all_to_all(jnp.stack([tokens] * lax.axis_size(('kv', 'tp'))), ('kv',...]
    all_to_all x0 -> x1, waiting for transfers between devices: none -> 2.48 us  [local(): lax.all_to_all(jnp.stack([tokens] * lax.axis_size(('kv', 'tp'))), ('kv',...]
    unnamed x25 -> x21, local copies, waits for them, and re-layouts: 3.18 us -> 5.31 us
    another operation x0 -> x1, local copies, waits for them, and re-layouts: none -> 1.46 us  [local(): jnp.stack([tokens] * lax.axis_size(('kv', 'tp')))]
  transfers between devices with their start and end apart: 1 -> 2, of which waited for: 1 -> 2; matrix products, arithmetic and copies ran while one was open for 1% -> 3% of each run, Pallas kernels for 0% -> 0%
where the time goes in v1:
time: 136 us
  blocking collectives  46.6 us (34%)
  waiting for transfers between devices  34.5 us (25%)
  matrix products  20.4 us (15%)
  between operations  14.8 us (11%)
  local copies, waits for them, and re-layouts  8.81 us (6%)
  starting transfers between devices  6.39 us (5%)
  other arithmetic  4.46 us (3%)
    unnamed x2, waiting for transfers between devices  32 us
    unnamed x2, blocking collectives  19.8 us
    all_gather x1, blocking collectives, local(): gathered = lax.all_gather(mixed, ('kv', 'tp'), axis=1, tiled=True)  14.1 us
    all_gather x1, blocking collectives, local(): every_head = lax.all_gather(gated[None], ('kv', 'tp'), axis=0, tiled=True)  12.8 us
    dot_general x1, matrix products, channel_mixer(): return jnp.dot(hidden, w_down, preferred_element_type=jnp.float32)  11 us
    all_to_all x1, starting transfers between devices, local(): lax.all_to_all(jnp.stack([tokens] * lax.axis_size(('kv', 'tp'))), ('kv',...  6.35 us
    dot_general x1, matrix products, channel_mixer(): gate_val = jnp.dot(normed, w_gate, preferred_element_type=jnp.float32)  5.9 us
    unnamed x21, local copies, waits for them, and re-layouts  5.31 us
  transfers between devices with their start and end apart: 2, of which 2 were waited for; matrix products, arithmetic and copies ran while one was open for 3% of the time, Pallas kernels for 0%

profile of v1, /device:TPU:0, one launch (start us, length us, event | category | flops | bytes accessed | tf_op | source)
XLA Modules:
  0.0 136.0 jit_solution(8624220324888958929)
XLA Ops:
  7.2 1.5 %stack.12 = bf16[8,4,512]{2,1,0:T(4,128)(2,1)} broadcast(bf16[4,512]{1,0:T(4,128)(2,1)} %param.14), dimensions={1,2} | broadcast | bytes 36864 | tf_op jit(solution)/shard_map/stack | solution.py:45
  8.6 6.4 %all-to-all-start = ((bf16[8,4,512]{2,1,0:T(4,128)(2,1)}), bf16[8,4,512]{2,1,0:T(4,128)(2,1)S(1)}, u32[]{:S(2)}, u32[]{:S(2)}) async-start(bf16[8,4,512]{2,1,0:T(4,128)(2,1)} %stack.12), calls=%async_computation | async-start | bytes 65536 | tf_op jit(solution)/shard_map/all_to_all | solution.py:45
  15.0 1.3 dynamic-slice.2
  16.3 1.3 dynamic-slice
  17.6 0.7 dynamic_slice.11
  18.3 2.5 %all-to-all-done = bf16[8,4,512]{2,1,0:T(4,128)(2,1)S(1)} async-done(((bf16[8,4,512]{2,1,0:T(4,128)(2,1)}), bf16[8,4,512]{2,1,0:T(4,128)(2,1)S(1)}, u32[]{:S(2)}, u32[]{:S(2)}) %all-to-all-start) | async-done | bytes 32800 | tf_op jit(solution)/shard_map/all_to_all | solution.py:45
  20.8 0.4 convolution_bitcast_fusion
  21.2 1.2 copy-done.1
  23.0 0.4 convolution_bitcast_fusion.2
  23.4 0.7 copy-done.3
  24.5 0.7 copy.21
  25.3 0.6 dynamic_slice.9
  26.6 32.0 %all-reduce.5.cloned.1.call-done = f32[4,4,1024]{2,1,0:T(4,128)} async-done(((f32[4,4,1024]{2,1,0:T(4,128)}), f32[4,4,1024]{2,1,0:T(4,128)}) %all-reduce.5.cloned.1.call-update) | async-done | bytes 65552
  58.6 1.5 %dynamic-slice_multiply_fusion = (f32[1,1,1024]{2,1,0:T(1,128)S(1)}, f32[1,1,1024]{2,1,0:T(1,128)S(1)}, f32[1,1,1024]{2,1,0:T(1,128)S(1)}, f32[1,1,1024]{2,1,0:T(1,128)S(1)}) fusion(f32[4,4,1024]{2,1,0:T(4,128)} %all-reduce.5.cloned.1.call-done, u32[]{:T(128)} %bitcast.22, u32[]{:T(128)S(6)} %convert.6, f32[]{:T(128)} %bitcast, u32[]{:T(128)S(6)} %convert.5, ...), kind=kLoop, calls=%fused_computation.26 | loop fusion | flops 7168 | bytes 32788 | tf_op jit(solution)/shard_map/mul | solution.py:69
  60.1 1.3 multiply_reduce_fusion
  61.6 12.8 %all-gather = bf16[8192]{0:T(1024)(128)(2,1)S(1)} all-gather(bf16[1024]{0:T(1024)(128)(2,1)S(1)} %fusion.13), channel_id=2, replica_groups=mesh['dp'=4,'kv'=4,'tp'=2] {'kv','tp'}, dimensions={0}, use_global_device_ids=true | all-gather | bytes 18432 | tf_op jit(solution)/shard_map/all_gather | solution.py:85
  74.4 2.0 %fusion.1 = bf16[4,512]{1,0:T(4,128)(2,1)S(1)} fusion(bf16[4,2048]{1,0:T(4,128)(2,1)S(1)} %reshape_transpose_reshape.3, bf16[2048,512]{1,0:T(8,128)(2,1)} %param.23, bf16[4,512]{1,0:T(4,128)(2,1)S(1)} %copy-done.6), kind=kOutput, calls=%fused_computation.8 | convolution fusion | flops 8394752 | bytes 2121728 | tf_op jit(solution)/shard_map/dot_general | solution.py:90
  76.4 14.1 %all_gather.7 = bf16[4,4096]{1,0:T(4,128)(2,1)S(1)} all-gather(bf16[4,512]{1,0:T(4,128)(2,1)S(1)} %fusion.1), channel_id=1, replica_groups=mesh['dp'=4,'kv'=4,'tp'=2] {'kv','tp'}, dimensions={1}, use_global_device_ids=true | all-gather | bytes 36864 | tf_op jit(solution)/shard_map/all_gather | solution.py:92
  90.6 5.9 %fusion.18 = f32[4,1408]{1,0:T(4,128)S(1)} fusion(bf16[4096,1408]{1,0:T(8,128)(2,1)} %param.25, bf16[4,4096]{1,0:T(4,128)(2,1)S(1)} %all_gather.7, f32[4096]{0:T(1024)S(1)} %copy-done.5, f32[4]{0:T(128)S(1)} %add_rsqrt_fusion), kind=kOutput, calls=%fused_computation.45 | convolution fusion | flops 46202880 | bytes 11606032 | tf_op jit(solution)/shard_map/dot_general | solution.py:14
  96.5 11.0 %convolution_convert_fusion = bf16[4,4096]{1,0:T(4,128)(2,1)S(1)} fusion(bf16[1408,4096]{1,0:T(8,128)(2,1)} %param.27, bf16[4096,1408]{1,0:T(8,128)(2,1)} %param.26, f32[4,1408]{1,0:T(4,128)S(1)} %fusion.18, bf16[4,4096]{1,0:T(4,128)(2,1)S(1)} %all_gather.7, f32[4096]{0:T(1024)S(1)} %copy-done.5, f32[4]{0:T(128)S(1)} %add_rsqrt_fusion), kind=kOutput, calls=%fused_computation | convolution fusion | flops 92390400 | bytes 23173136 | tf_op jit(solution)/shard_map/dot_general | solution.py:17
  107.5 3.6 %all-reduce.1 = bf16[4,4,2,512]{3,0,2,1:T(4,128)(2,1)S(1)} all-reduce(bf16[4,4,2,512]{3,0,2,1:T(4,128)(2,1)S(1)} %bitcast.52), channel_id=4, replica_groups=mesh['dp'=4,'kv'=4,'tp'=2] {'tp'}, use_global_device_ids=true, to_apply=%region_5.6.clone | all-reduce | flops 16384 | bytes 65536
  111.1 0.6 constant_dynamic-slice_fusion
  111.8 16.2 %all-reduce.2 = bf16[4,4,1,512]{3,0,2,1:T(4,128)(2,1)S(1)} all-reduce(bf16[4,4,1,512]{3,0,2,1:T(4,128)(2,1)S(1)} %constant_dynamic-slice_fusion), channel_id=5, replica_groups=mesh['dp'=4,'kv'=4,'tp'=2] {'kv'}, use_global_device_ids=true, to_apply=%region_6.7.clone | all-reduce | flops 8192 | bytes 32768
  127.9 1.2 fusion.9
  (33 shorter events, 1.7 us)
Async XLA Ops:
  7.2 13.6 %copy-start = (bf16[1024,1024]{1,0:T(8,128)(2,1)S(1)}, bf16[1024,1024]{1,0:T(8,128)(2,1)}, u32[]{:S(2)}) copy-start(bf16[1024,1024]{1,0:T(8,128)(2,1)} %param.20) | copy-start | bytes 6291460
  8.6 12.1 %all-to-all-start = ((bf16[8,4,512]{2,1,0:T(4,128)(2,1)}), bf16[8,4,512]{2,1,0:T(4,128)(2,1)S(1)}, u32[]{:S(2)}, u32[]{:S(2)}) async-start(bf16[8,4,512]{2,1,0:T(4,128)(2,1)} %stack.12), calls=%async_computation | async-start | bytes 65536 | tf_op jit(solution)/shard_map/all_to_all | solution.py:45
  15.0 43.6 %all-reduce.5.cloned.1.call-start = ((), (), s32[]{:S(2)}) async-start(), calls=%async_computation.1 | async-start | bytes 131072
  20.7 1.6 %copy-start.1 = (bf16[1024,1024]{1,0:T(8,128)(2,1)S(1)}, bf16[1024,1024]{1,0:T(8,128)(2,1)}, u32[]{:S(2)}) copy-start(bf16[1024,1024]{1,0:T(8,128)(2,1)} %param.19) | copy-start | bytes 6291460
  20.8 2.2 %copy-start.2 = (bf16[1024,1024]{1,0:T(8,128)(2,1)S(1)}, bf16[1024,1024]{1,0:T(8,128)(2,1)}, u32[]{:S(2)}) copy-start(bf16[1024,1024]{1,0:T(8,128)(2,1)} %param.18) | copy-start | bytes 6291460
  22.3 1.7 %copy-start.3 = (bf16[1024,1024]{1,0:T(8,128)(2,1)S(1)}, bf16[1024,1024]{1,0:T(8,128)(2,1)}, u32[]{:S(2)}) copy-start(bf16[1024,1024]{1,0:T(8,128)(2,1)} %param.17) | copy-start | bytes 6291460
  23.0 37.1 %copy-start.7 = (f32[1024]{0:T(1024)S(1)}, f32[1024]{0:T(1024)}, u32[]{:S(2)}) copy-start(f32[1024]{0:T(1024)} %param.21) | copy-start | bytes 12292
  23.0 37.2 %copy-start.4 = (f32[1,8,128,128]{3,2,1,0:T(8,128)S(1)}, f32[1,8,128,128]{3,2,1,0:T(8,128)}, u32[]{:S(2)}) copy-start(f32[1,8,128,128]{3,2,1,0:T(8,128)} %param.15) | copy-start | bytes 1572868
  24.1 37.5 %copy-start.8 = (f32[1024]{0:T(1024)S(1)}, f32[1024]{0:T(1024)}, u32[]{:S(2)}) copy-start(f32[1024]{0:T(1024)} %param.22) | copy-start | bytes 12292
  24.1 50.3 %copy-start.6 = (bf16[4,512]{1,0:T(4,128)(2,1)S(1)}, bf16[4,512]{1,0:T(4,128)(2,1)}, u32[]{:S(2)}) copy-start(bf16[4,512]{1,0:T(4,128)(2,1)} %param.14) | copy-start | bytes 12292
  24.5 66.2 %copy-start.5 = (f32[4096]{0:T(1024)S(1)}, f32[4096]{0:T(1024)}, u32[]{:S(2)}) copy-start(f32[4096]{0:T(1024)} %param.24) | copy-start | bytes 49156
Sparse Core Ops, SparseCore 0:
  25.3 33.2 all-reduce.4
